TPU v7x, 32 devices: a whole 2x2x4 slice. The times are simulated.
32 devices in a mesh: ep: 16 (over z, y, x), tp: 2 (over core).
Axes of the slice: x: 2, y: 2, z: 4, core: 2. Of those that a mesh axis runs over, the one named last changes fastest.
Arguments:
- tokens: bfloat16 [112, 2304], P('ep'), may hold values from -6 to 6
- attn_gain: bfloat16 [2304], replicated, may hold values from 0.099609375 to 1.8984375
- query_weight: bfloat16 [2304, 2048], P(None, 'tp'), may hold values from -0.125 to 0.125
- key_weight: bfloat16 [2304, 2048], P(None, 'tp'), may hold values from -0.125 to 0.125
- value_weight: bfloat16 [2304, 2048], P(None, 'tp'), may hold values from -0.125 to 0.125
- out_weight: bfloat16 [2304, 2048], P(None, 'tp'), may hold values from -0.125 to 0.125
- lambdas: float32 [16], P('tp'), may hold values from 0.3 to 0.8
- head_gain: bfloat16 [128], replicated, may hold values from 0.099609375 to 1.8984375
- cache_keys: bfloat16 [112, 1024, 16, 128], P('ep', None, 'tp'), may hold values from -1500 to 1500
- cache_values: bfloat16 [112, 1024, 16, 128], P('ep', None, 'tp'), may hold values from -6 to 6
- lengths: int32 [112], P('ep'), may hold values from 2 to 1024, as said below
- moe_gain: bfloat16 [2304], replicated, may hold values from 0.099609375 to 1.8984375
- gate_weight: bfloat16 [16, 2304, 1024], P('ep', None, 'tp'), may hold values from -0.125 to 0.125
- up_weight: bfloat16 [16, 2304, 1024], P('ep', None, 'tp'), may hold values from -0.125 to 0.125
- down_weight: bfloat16 [16, 1024, 2304], P('ep', 'tp'), may hold values from -0.1875 to 0.1875
- shared_gate: bfloat16 [2304, 1024], P(None, 'tp'), may hold values from -0.125 to 0.125
- shared_up: bfloat16 [2304, 1024], P(None, 'tp'), may hold values from -0.125 to 0.125
- shared_down: bfloat16 [1024, 2304], P('tp'), may hold values from -0.1875 to 0.1875
- expert_ids: int32 [112, 6], P('ep'), may hold values from 0 to 15, all different within a row; in each aligned block of 7 rows (0 to 6, 7 to 13, ...) at most 5 rows name the same one
- expert_weights: float32 [112, 6], P('ep'), may hold values from 0.2 to 1
Outputs:
- result: bfloat16 [112, 2304], P('ep', 'tp')
Inputs may be any that keep to these rules, and one draw needn't show every extreme that they name: `expert_ids`: each row names 6 different experts. Among the rows of one device (aligned blocks of 7 rows) no expert is named by more than 5 rows, a bound that some block reaches. `lengths`: some sequence has 1024 cached positions.
All inputs are finite; a program needn't handle non-finite values.
Results may differ from a plain program's by a relative error of at most 0.02.
Values may be sent and summed in bfloat16 or wider, within the bound.
No kernel may reach another device: no remote copies, remote signals or barrier semaphores. Data moves between devices by JAX's collectives and lax.ppermute only.
A program may use at most 128 MiB of HBM per device.

v0:
```python
import jax
import jax.numpy as jnp
from jax import lax
from jax.experimental import pallas as pl
from jax.experimental.pallas import tpu as pltpu
from jax.sharding import PartitionSpec as P

epsilon = 1e-06
GRAIN = 128
CHUNK = 1024
PIECES = 1
FLIGHT = 3
AHEAD = 7
OUT_AT = 1
SHARES_FLOPS = 4_000_000_000


def rms_scale(values, gain):
    wide = values.astype(jnp.float32)
    return (
        wide
        * lax.rsqrt(jnp.mean(wide * wide, axis=-1, keepdims=True) + epsilon)
        * gain.astype(jnp.float32)
    )


def attend_body(
    lengths_hbm,
    lambdas_hbm,
    tokens_hbm,
    attn_gain_hbm,
    head_gain_hbm,
    query_hbm,
    key_hbm,
    value_hbm,
    out_hbm,
    keys_hbm,
    values_hbm,
    part_out,
    lengths,
    lambdas,
    tokens,
    attn_gain,
    head_gain,
    query_w,
    key_w,
    value_w,
    out_w,
    keys,
    values,
    scores,
    peaks,
    own_scores,
    queries,
    new_keys,
    new_values,
    head_outs,
    head_rows,
    small_sems,
    weight_sems,
    key_sems,
    value_sems,
):
    seq_dev = tokens.shape[0]
    heads = queries.shape[1]
    width = queries.shape[2]
    head_dim = width // 2
    cache_rows = keys.shape[1]
    scale = head_dim ** (-0.5)
    grain_rows = GRAIN * heads
    span = query_w.shape[0] // PIECES

    def weight_copy(i, piece):
        source = (query_hbm, key_hbm, value_hbm, out_hbm)[i]
        target = (query_w, key_w, value_w, out_w)[i]
        rows = pl.ds(piece * span, span)
        return pltpu.make_async_copy(source.at[rows], target.at[rows], weight_sems.at[i, piece])

    def live_rows(s):
        return pl.multiple_of((lengths[s] + GRAIN - 1) // GRAIN * grain_rows, grain_rows)

    def key_copy(s):
        rows = pl.ds(0, live_rows(s))
        return pltpu.make_async_copy(keys_hbm.at[s, rows], keys.at[s, rows], key_sems.at[s])

    def value_copy(s):
        rows = pl.ds(0, live_rows(s))
        return pltpu.make_async_copy(values_hbm.at[s, rows], values.at[s, rows], value_sems.at[s])

    small = [
        pltpu.make_async_copy(source, target, small_sems.at[i])
        for i, (source, target) in enumerate(
            (
                (lengths_hbm, lengths),
                (lambdas_hbm, lambdas),
                (tokens_hbm, tokens),
                (attn_gain_hbm, attn_gain),
                (head_gain_hbm, head_gain),
            )
        )
    ]
    for copy in small:
        copy.start()
    queue = [(weight_copy, (i, piece)) for i in range(3) for piece in range(PIECES)]
    for s in range(AHEAD):
        queue += [(key_copy, (s,)), (value_copy, (s,))]

    def start_next():
        if queue:
            make, where = queue.pop(0)
            make(*where).start()

    for _ in range(FLIGHT):
        start_next()
    for copy in small:
        copy.wait()

    def clear_tail(s, carry):
        def clear(g, carry):
            rows = pl.ds(pl.multiple_of(g * grain_rows, grain_rows), grain_rows)
            keys[s, rows, :] = jnp.zeros((grain_rows, width), jnp.bfloat16)
            values[s, rows, :] = jnp.zeros((grain_rows, width), jnp.bfloat16)
            return carry

        used = jnp.where(lengths[s] > cache_rows // heads // 2, cache_rows, cache_rows // 2)
        return lax.fori_loop(live_rows(s) // grain_rows, used // grain_rows, clear, carry)

    lax.fori_loop(0, seq_dev, clear_tail, 0)

    normed = rms_scale(tokens[...], attn_gain[...].astype(jnp.float32).reshape(1, -1)).astype(jnp.bfloat16)
    for i, (weight, target) in enumerate(
        ((query_w, queries), (key_w, new_keys), (value_w, new_values))
    ):
        rows = None
        for piece in range(PIECES):
            weight_copy(i, piece).wait()
            start_next()
            lines = slice(piece * span, (piece + 1) * span)
            more = jnp.dot(normed[:, lines], weight[lines, :], preferred_element_type=jnp.float32)
            rows = more if rows is None else rows + more
        rows = rows.astype(jnp.bfloat16).astype(jnp.float32)
        for s in range(seq_dev):
            for h in range(heads):
                target[s, h : h + 1, :] = rows[s : s + 1, h * width : (h + 1) * width]

    while queue:
        start_next()
    lane = lax.broadcasted_iota(jnp.int32, (2 * heads, width), 1)
    row = lax.broadcasted_iota(jnp.int32, (2 * heads, width), 0)
    map_mask = (lane < head_dim) == (row < heads)
    lane_or_far = jnp.where(lane % heads == row % heads, lane, jnp.int32(1 << 30))
    head_row = lax.broadcasted_iota(jnp.int32, (heads, 1), 0)
    lam = jnp.zeros((heads, 1), jnp.float32)
    for h in range(heads):
        lam = jnp.where(head_row == h, lambdas[h], lam)

    def score_stage(s, size):
        slot = s % 2
        live = lengths[s] * heads
        query = queries[s]
        query16 = jnp.where(map_mask, jnp.concatenate([query, query], axis=0), 0.0)
        fresh = new_keys[s]
        fresh16 = jnp.concatenate([fresh, fresh], axis=0)
        own = jnp.sum(query16 * fresh16, axis=1, keepdims=True) * scale
        query16 = (query16 * scale).astype(jnp.bfloat16)
        none = jnp.zeros_like(query16)
        query32 = jnp.concatenate(
            [
                jnp.concatenate([query16, none], axis=1),
                jnp.concatenate([none, query16], axis=1),
            ],
            axis=0,
        )
        half = size * heads // 2
        peak = jnp.full((2 * heads, width), -jnp.inf, jnp.float32)
        for c in range(0, half, CHUNK):
            pair = jnp.concatenate(
                [keys[s, c : c + CHUNK, :], keys[s, half + c : half + c + CHUNK, :]], axis=1
            )
            block = lax.dot_general(
                query32, pair, (((1,), (1,)), ((), ())), preferred_element_type=jnp.float32
            )
            for part in range(2):
                for j in range(0, CHUNK, width):
                    start = part * half + c + j
                    tile = block[part * 2 * heads : (part + 1) * 2 * heads, j : j + width]
                    tile = jnp.where(lane_or_far < live - start, tile, -jnp.inf)
                    scores[slot, :, start : start + width] = tile
                    peak = jnp.maximum(peak, tile)
        peak = jnp.maximum(jnp.max(peak, axis=1, keepdims=True), own)
        peaks[slot] = jnp.broadcast_to(peak, (2 * heads, width))
        own_scores[slot] = jnp.broadcast_to(own, (2 * heads, width))

    def value_stage(s, size):
        slot = s % 2
        rows = size * heads
        half = rows // 2
        peak = peaks[slot]
        own_term = jnp.exp(own_scores[slot] - peak)
        sums = [jnp.zeros((2 * heads, width), jnp.float32) for _ in range(4)]
        for i, start in enumerate(range(0, rows, width)):
            tile = jnp.exp(scores[slot, :, start : start + width] - peak)
            scores[slot, :, start : start + width] = tile
            sums[i % 4] = sums[i % 4] + tile
        total = (sums[0] + sums[1]) + (sums[2] + sums[3])
        inverse = 1.0 / (jnp.sum(total, axis=1, keepdims=True) + own_term)
        first = inverse[:heads]
        second = lam * inverse[heads:]
        acc = jnp.zeros((2 * heads, 2 * width), jnp.float32)
        for c in range(0, half, CHUNK):
            tiles = []
            for j in range(c, c + CHUNK, width):
                mixed = [
                    scores[slot, :heads, start : start + width] * first
                    - scores[slot, heads:, start : start + width] * second
                    for start in (j, half + j)
                ]
                tiles.append(jnp.concatenate(mixed, axis=0).astype(jnp.bfloat16))
            pair = jnp.concatenate(
                [values[s, c : c + CHUNK, :], values[s, half + c : half + c + CHUNK, :]], axis=1
            )
            acc = acc + jnp.dot(
                jnp.concatenate(tiles, axis=1), pair, preferred_element_type=jnp.float32
            )
        own_mixture = own_term[:heads] * first - own_term[heads:] * second
        own_mixture = own_mixture.astype(jnp.bfloat16).astype(jnp.float32)
        head_outs[s] = acc[:heads, :width] + acc[heads:, width:] + own_mixture * new_values[s]

    full = cache_rows // heads
    sizes = (full // 2, full)

    def sized(run, s):
        for size in sizes:

            @pl.when((lengths[s] > sizes[0]) == (size == full))
            def _():
                run(s, size)

    key_copy(0).wait()
    sized(score_stage, 0)

    def stage(s, carry):
        key_copy(s).wait()
        value_copy(s - 1).wait()

        @pl.when(s + AHEAD - 1 < seq_dev)
        def _():
            key_copy(s + AHEAD - 1).start()
            value_copy(s + AHEAD - 1).start()

        @pl.when(s == OUT_AT)
        def _():
            for piece in range(PIECES):
                weight_copy(3, piece).start()

        sized(score_stage, s)
        sized(value_stage, s - 1)
        return carry

    lax.fori_loop(1, seq_dev, stage, 0)
    value_copy(seq_dev - 1).wait()
    sized(value_stage, seq_dev - 1)
    head_normed = rms_scale(head_outs[...], head_gain[...].reshape(1, 1, width))
    for s in range(seq_dev):
        for h in range(heads):
            head_rows[s : s + 1, h * width : (h + 1) * width] = head_normed[s, h : h + 1, :]
    for piece in range(PIECES):
        weight_copy(3, piece).wait()
    part = lax.dot_general(
        head_rows[:seq_dev, :].astype(jnp.bfloat16),
        out_w[...],
        (((1,), (1,)), ((), ())),
        preferred_element_type=jnp.float32,
    )
    part_out[...] = part.astype(jnp.bfloat16)


def attend_kernel(
    tokens,
    attn_gain,
    query_weight,
    key_weight,
    value_weight,
    out_weight,
    lambdas,
    head_gain,
    cache_keys,
    cache_values,
    lengths,
):
    seq_dev, model_width = tokens.shape
    _, cache_len, heads, width = cache_keys.shape
    cols = heads * width
    rows = cache_len * heads
    vmem = pl.BlockSpec(memory_space=pltpu.VMEM)
    anywhere = pl.BlockSpec(memory_space=pltpu.HBM)
    bf16, f32 = jnp.bfloat16, jnp.float32
    return pl.pallas_call(
        attend_body,
        out_shape=jax.ShapeDtypeStruct((seq_dev, model_width), bf16),
        in_specs=[anywhere] * 11,
        out_specs=vmem,
        scratch_shapes=[
            pltpu.SMEM((seq_dev,), jnp.int32),
            pltpu.SMEM((heads,), f32),
            pltpu.VMEM((seq_dev, model_width), bf16),
            pltpu.VMEM((model_width,), bf16),
            pltpu.VMEM((1, width), bf16),
            pltpu.VMEM((model_width, cols), bf16),
            pltpu.VMEM((model_width, cols), bf16),
            pltpu.VMEM((model_width, cols), bf16),
            pltpu.VMEM((model_width, cols), bf16),
            pltpu.VMEM((seq_dev, rows, width), bf16),
            pltpu.VMEM((seq_dev, rows, width), bf16),
            pltpu.VMEM((2, 2 * heads, rows), f32),
            pltpu.VMEM((2, 2 * heads, width), f32),
            pltpu.VMEM((2, 2 * heads, width), f32),
            pltpu.VMEM((seq_dev, heads, width), f32),
            pltpu.VMEM((seq_dev, heads, width), f32),
            pltpu.VMEM((seq_dev, heads, width), f32),
            pltpu.VMEM((seq_dev, heads, width), f32),
            pltpu.VMEM((seq_dev + 1, cols), f32),
            pltpu.SemaphoreType.DMA((5,)),
            pltpu.SemaphoreType.DMA((4, PIECES)),
            pltpu.SemaphoreType.DMA((seq_dev,)),
            pltpu.SemaphoreType.DMA((seq_dev,)),
        ],
        compiler_params=pltpu.CompilerParams(vmem_limit_bytes=54 << 20),
        name="attend",
    )(
        lengths,
        lambdas,
        tokens,
        attn_gain,
        head_gain.reshape(1, -1),
        query_weight,
        key_weight,
        value_weight,
        out_weight,
        cache_keys.reshape(seq_dev, rows, width),
        cache_values.reshape(seq_dev, rows, width),
    )


def slot_map(shape, cap, rows_at, slots_at):
    packed = lax.broadcasted_iota(jnp.int32, shape, rows_at)
    padded = lax.broadcasted_iota(jnp.int32, shape, slots_at)
    rank = jnp.full(shape, -7, jnp.int32)
    place = jnp.full(shape, -9, jnp.int32)
    for c in range(shape[slots_at] // 8):
        inside = (packed >= c * cap) & (packed < (c + 1) * cap)
        inside = inside & (padded >= c * 8) & (padded < (c + 1) * 8)
        rank = jnp.where(inside, packed - c * cap, rank)
        place = jnp.where(inside, padded - c * 8, place)
    return rank.astype(jnp.float32), place.astype(jnp.float32)


def slot_codes(ids, experts):
    seq_dev, top_count = ids.shape
    expert = lax.broadcasted_iota(jnp.int32, (seq_dev, experts), 1)
    hits = jnp.zeros((seq_dev, experts), jnp.float32)
    for k in range(top_count):
        hits = hits + jnp.where(ids[:, k : k + 1] == expert, 1.0, 0.0)
    earlier = lax.broadcasted_iota(jnp.int32, (seq_dev, seq_dev), 0)
    earlier = earlier > lax.broadcasted_iota(jnp.int32, (seq_dev, seq_dev), 1)
    rank = jnp.dot(
        jnp.where(earlier, 1.0, 0.0).astype(jnp.bfloat16),
        hits.astype(jnp.bfloat16),
        preferred_element_type=jnp.float32,
    )
    return jnp.where(hits > 0.5, rank, -1.0)


def padded_rows(rows, value):
    seq_dev, cols = rows.shape
    if seq_dev == 8:
        return rows
    return jnp.concatenate([rows, jnp.full((8 - seq_dev, cols), value, rows.dtype)], axis=0)


def prepare_body(index, tokens, own_part, other_part, gain, ids, mixed_out, normed_out, send_out):
    experts, block, lanes = send_out.shape
    cols = tokens.shape[1] // 2
    chunks = cols // lanes
    cap = capacity_of(tokens.shape[0], ids.shape[1], experts)
    total = own_part[...].astype(jnp.float32) + other_part[...].astype(jnp.float32)
    mixed = (tokens[...].astype(jnp.float32) + total).astype(jnp.bfloat16)
    mixed_out[...] = mixed
    normed = rms_scale(mixed, gain[...]).astype(jnp.bfloat16)
    normed_out[...] = normed
    codes = padded_rows(slot_codes(ids[...], experts), -1.0)
    codes = jnp.concatenate([codes] * chunks, axis=0)
    expert = lax.broadcasted_iota(jnp.int32, (experts, experts), 0)
    eye = expert == lax.broadcasted_iota(jnp.int32, (experts, experts), 1)
    code_rows = lax.dot_general(
        jnp.where(eye, 1.0, 0.0).astype(jnp.bfloat16),
        codes.astype(jnp.bfloat16),
        (((1,), (1,)), ((), ())),
        preferred_element_type=jnp.float32,
    )
    rank, _ = slot_map((block, chunks * 8), cap, 0, 1)
    picks = [jnp.where(code_rows[e : e + 1, :] == rank, 1.0, 0.0) for e in range(experts)]
    picks = jnp.concatenate(picks, axis=0).astype(jnp.bfloat16)
    wide = padded_rows(normed.astype(jnp.float32), 0.0)
    low = index[0] == 0
    stack = [
        jnp.where(
            low, wide[:, c * lanes : (c + 1) * lanes], wide[:, cols + c * lanes : cols + (c + 1) * lanes]
        )
        for c in range(chunks)
    ]
    stack = jnp.concatenate(stack, axis=0).astype(jnp.bfloat16)
    send = jnp.dot(picks, stack, preferred_element_type=jnp.float32).astype(jnp.bfloat16)
    for e in range(experts):
        send_out[e] = send[e * block : (e + 1) * block]


def shares_body(ids, weights, after, high_out, low_out):
    experts, padded, block = high_out.shape
    chunks = padded // 8
    seq_dev, top_count = ids.shape
    cap = capacity_of(seq_dev, top_count, experts)
    codes = padded_rows(slot_codes(ids[...], experts), -1.0)
    expert = lax.broadcasted_iota(jnp.int32, (seq_dev, experts), 1)
    shares = jnp.zeros((seq_dev, experts), jnp.float32)
    for k in range(top_count):
        shares = shares + jnp.where(ids[:, k : k + 1] == expert, weights[:, k : k + 1], 0.0)
    codes = jnp.concatenate([codes] * chunks, axis=0)
    shares = jnp.concatenate([padded_rows(shares, 0.0)] * chunks, axis=0)
    rank, _ = slot_map((padded, block), cap, 1, 0)
    for e in range(experts):
        share = jnp.where(codes[:, e : e + 1] == rank, shares[:, e : e + 1], 0.0)
        high = share.astype(jnp.bfloat16)
        high_out[e] = high
        low_out[e] = (share - high.astype(jnp.float32)).astype(jnp.bfloat16)


def expert_body(
    index, own, other, gate_hbm, up_hbm, down_hbm, own_out, sent_out, rows, gate, up, down, sems
):
    pairs = ((gate_hbm, gate), (up_hbm, up), (down_hbm, down))
    copies = [pltpu.make_async_copy(a, b, sems.at[i]) for i, (a, b) in enumerate(pairs)]
    for copy in copies:
        copy.start()
    experts, block, lanes = own.shape
    cols = rows.shape[1] // 2
    chunks = cols // lanes
    cap = block_cap(block, chunks)
    tp = index[0]
    rank, place = slot_map((chunks * 8, block), cap, 1, 0)
    spread = jnp.where(rank == place, 1.0, 0.0).astype(jnp.bfloat16)
    rank, place = slot_map((block, chunks * 8), cap, 0, 1)
    gather = jnp.where(rank == place, 1.0, 0.0).astype(jnp.bfloat16)
    for source, half in ((own, tp), (other, 1 - tp)):
        start = half * cols
        for e in range(experts):
            got = jnp.dot(spread, source[e], preferred_element_type=jnp.float32)
            for c in range(chunks):
                at = pl.ds(pl.multiple_of(start + c * lanes, lanes), lanes)
                rows[e * 8 : (e + 1) * 8, at] = got[c * 8 : (c + 1) * 8]
    x = rows[...].astype(jnp.bfloat16)
    copies[0].wait()
    gate_part = jnp.dot(x, gate[...], preferred_element_type=jnp.float32)
    copies[1].wait()
    up_part = jnp.dot(x, up[...], preferred_element_type=jnp.float32)
    hidden = (gate_part / (1.0 + jnp.exp(-gate_part)) * up_part).astype(jnp.bfloat16)
    copies[2].wait()
    rows[...] = jnp.dot(hidden, down[...], preferred_element_type=jnp.float32)
    for target, half in ((sent_out, 1 - tp), (own_out, tp)):
        start = half * cols
        for e in range(experts):
            tiles = [
                rows[e * 8 : (e + 1) * 8, pl.ds(pl.multiple_of(start + c * lanes, lanes), lanes)]
                for c in range(chunks)
            ]
            tiles = jnp.concatenate(tiles, axis=0).astype(jnp.bfloat16)
            packed = jnp.dot(gather, tiles, preferred_element_type=jnp.float32)
            target[e] = packed.astype(jnp.bfloat16)


def combine_body(index, returned, high, low, mixed, own_shared, other_shared, result):
    experts, block, lanes = returned.shape
    cols = result.shape[1]
    seq_dev = result.shape[0]
    acc = jnp.zeros((high.shape[1], lanes), jnp.float32)
    for e in range(experts):
        acc = acc + jnp.dot(high[e], returned[e], preferred_element_type=jnp.float32)
        acc = acc + jnp.dot(low[e], returned[e], preferred_element_type=jnp.float32)
    first = index[0] == 0
    for c in range(cols // lanes):
        left = slice(c * lanes, (c + 1) * lanes)
        right = slice(cols + c * lanes, cols + (c + 1) * lanes)
        kept = jnp.where(first, mixed[:, left].astype(jnp.float32), mixed[:, right].astype(jnp.float32))
        own = jnp.where(
            first, own_shared[:, left].astype(jnp.float32), own_shared[:, right].astype(jnp.float32)
        )
        shared = own + other_shared[:, left].astype(jnp.float32)
        total = kept + acc[c * 8 : c * 8 + seq_dev] + shared
        result[:, left] = total.astype(jnp.bfloat16)


def capacity_of(seq_dev, top_count, experts):
    return min(seq_dev, max(2, 2 * seq_dev * top_count // experts))


def block_cap(block, chunks):
    return block // chunks


def routed_pair(
    tokens,
    attn_part,
    moe_gain,
    gate_weight,
    up_weight,
    down_weight,
    shared_gate,
    shared_up,
    shared_down,
    expert_ids,
    expert_weights,
):
    seq_dev, model_width = tokens.shape
    experts = lax.axis_size("ep")
    cols = model_width // 2
    lanes = 128
    chunks = cols // lanes
    cap = capacity_of(seq_dev, expert_ids.shape[1], experts)
    block = (cap * chunks + 15) // 16 * 16
    bf16 = jnp.bfloat16
    vmem = pl.BlockSpec(memory_space=pltpu.VMEM)
    smem = pl.BlockSpec(memory_space=pltpu.SMEM)
    anywhere = pl.BlockSpec(memory_space=pltpu.HBM)
    swap = [(0, 1), (1, 0)]
    index = lax.axis_index("tp").astype(jnp.int32).reshape(1)
    other_part = lax.ppermute(attn_part, "tp", swap)
    shape = jax.ShapeDtypeStruct
    packed = shape((experts, block, lanes), bf16)
    rows = shape((seq_dev, model_width), bf16)
    mixed, normed, send = pl.pallas_call(
        prepare_body,
        out_shape=(rows, rows, packed),
        in_specs=[smem] + [vmem] * 5,
        out_specs=(vmem,) * 3,
        compiler_params=pltpu.CompilerParams(vmem_limit_bytes=8 << 20),
        name="prepare",
    )(index, tokens, attn_part, other_part, moe_gain.reshape(1, -1), expert_ids)
    arrived = lax.all_to_all(send, "ep", split_axis=0, concat_axis=0, tiled=True)
    hidden = gate_weight.shape[2]
    mix = shape((experts, chunks * 8, block), bf16)
    high, low = pl.pallas_call(
        shares_body,
        out_shape=(mix, mix),
        in_specs=[vmem, vmem, anywhere],
        out_specs=(vmem,) * 2,
        compiler_params=pltpu.CompilerParams(vmem_limit_bytes=8 << 20),
        cost_estimate=pl.CostEstimate(
            flops=SHARES_FLOPS, transcendentals=0, bytes_accessed=4 * experts * chunks * 8 * block
        ),
        name="shares",
    )(expert_ids, expert_weights, normed)
    arrived, high = lax.optimization_barrier((arrived, high))
    partner = lax.ppermute(arrived, "tp", swap)
    own_out, sent_out = pl.pallas_call(
        expert_body,
        out_shape=(packed, packed),
        in_specs=[smem] + [vmem] * 2 + [anywhere] * 3,
        out_specs=(vmem,) * 2,
        scratch_shapes=[
            pltpu.VMEM((experts * 8, model_width), jnp.float32),
            pltpu.VMEM((model_width, hidden), bf16),
            pltpu.VMEM((model_width, hidden), bf16),
            pltpu.VMEM((hidden, model_width), bf16),
            pltpu.SemaphoreType.DMA((3,)),
        ],
        compiler_params=pltpu.CompilerParams(vmem_limit_bytes=24 << 20),
        name="expert",
    )(
        index,
        arrived,
        partner,
        *(
            pltpu.with_memory_space_constraint(weight[0], pltpu.HBM)
            for weight in (gate_weight, up_weight, down_weight)
        ),
    )
    expert_sum = own_out.astype(jnp.float32) + lax.ppermute(sent_out, "tp", swap).astype(jnp.float32)
    returned = lax.all_to_all(
        expert_sum.astype(bf16), "ep", split_axis=0, concat_axis=0, tiled=True
    )
    shared_gate_out = jnp.dot(normed, shared_gate, preferred_element_type=jnp.float32)
    shared_up_out = jnp.dot(normed, shared_up, preferred_element_type=jnp.float32)
    shared_hidden = (jax.nn.silu(shared_gate_out) * shared_up_out).astype(bf16)
    shared_part = jnp.dot(shared_hidden, shared_down, preferred_element_type=jnp.float32)
    shared_part = shared_part.astype(bf16)
    shared_sent = lax.dynamic_slice_in_dim(shared_part, (1 - index[0]) * cols, cols, 1)
    shared_other = lax.ppermute(shared_sent, "tp", swap)
    return pl.pallas_call(
        combine_body,
        out_shape=shape((seq_dev, cols), bf16),
        in_specs=[smem] + [vmem] * 6,
        out_specs=vmem,
        compiler_params=pltpu.CompilerParams(vmem_limit_bytes=8 << 20),
        name="combine",
    )(index, returned, high, low, mixed, shared_part, shared_other)


def attend_plain(
    tokens,
    attn_gain,
    query_weight,
    key_weight,
    value_weight,
    out_weight,
    lambdas,
    head_gain,
    cache_keys,
    cache_values,
    lengths,
):
    seq_dev, model_width = tokens.shape
    local_heads = lambdas.shape[0]
    head_dim = cache_keys.shape[-1] // 2
    cache_len = cache_keys.shape[1]
    normed = rms_scale(tokens, attn_gain).astype(jnp.bfloat16)
    query_rows = jnp.dot(normed, query_weight, preferred_element_type=jnp.float32).astype(
        jnp.bfloat16
    )
    key_new = jnp.dot(normed, key_weight, preferred_element_type=jnp.float32).astype(jnp.bfloat16)
    value_new = jnp.dot(normed, value_weight, preferred_element_type=jnp.float32).astype(
        jnp.bfloat16
    )
    score_scale = head_dim ** (-0.5)
    queries = query_rows.reshape(seq_dev, local_heads, 2, head_dim)
    new_keys = key_new.reshape(seq_dev, local_heads, 2, head_dim)
    new_values = value_new.reshape(seq_dev, local_heads, 2 * head_dim)
    past_keys = cache_keys.reshape(seq_dev, cache_len, local_heads, 2, head_dim)
    scores = (
        jnp.einsum("shmd,sjhmd->shmj", queries, past_keys, preferred_element_type=jnp.float32)
        * score_scale
    )
    own_score = (
        jnp.sum(queries.astype(jnp.float32) * new_keys.astype(jnp.float32), axis=-1) * score_scale
    )
    live_mask = (jnp.arange(cache_len, dtype=jnp.int32)[None, :] < lengths[:, None])[
        :, None, None, :
    ]
    peak_score = jnp.maximum(jnp.max(jnp.where(live_mask, scores, -jnp.inf), axis=-1), own_score)
    exp_terms = jnp.where(live_mask, jnp.exp(scores - peak_score[..., None]), 0.0)
    own_term = jnp.exp(own_score - peak_score)
    denom_sum = jnp.sum(exp_terms, axis=-1) + own_term
    map_probs = exp_terms / denom_sum[..., None]
    own_prob = own_term / denom_sum
    lambda_row = lambdas[None, :]
    mixture = (map_probs[:, :, 0] - lambda_row[..., None] * map_probs[:, :, 1]).astype(jnp.bfloat16)
    own_mixture = (own_prob[:, :, 0] - lambda_row * own_prob[:, :, 1]).astype(jnp.bfloat16)
    head_out = jnp.einsum(
        "shj,sjhv->shv", mixture, cache_values, preferred_element_type=jnp.float32
    )
    head_out = head_out + own_mixture.astype(jnp.float32)[..., None] * new_values.astype(
        jnp.float32
    )
    head_normed = (
        rms_scale(head_out, head_gain)
        .astype(jnp.bfloat16)
        .reshape(seq_dev, local_heads * 2 * head_dim)
    )
    return lax.dot_general(
        head_normed, out_weight, (((1,), (1,)), ((), ())), preferred_element_type=jnp.float32
    ).astype(jnp.bfloat16)


def scatter_sum(part):
    part = part.astype(jnp.bfloat16)
    if lax.axis_size("tp") != 2:
        return lax.psum_scatter(part, "tp", scatter_dimension=1, tiled=True).astype(jnp.float32)
    cols = part.shape[1] // 2
    index = lax.axis_index("tp")
    own = lax.dynamic_slice_in_dim(part, index * cols, cols, 1)
    sent = lax.dynamic_slice_in_dim(part, (1 - index) * cols, cols, 1)
    arrived = lax.ppermute(sent, "tp", [(0, 1), (1, 0)])
    return own.astype(jnp.float32) + arrived.astype(jnp.float32)


def shards(
    tokens,
    attn_gain,
    query_weight,
    key_weight,
    value_weight,
    out_weight,
    lambdas,
    head_gain,
    cache_keys,
    cache_values,
    lengths,
    moe_gain,
    gate_weight,
    up_weight,
    down_weight,
    shared_gate,
    shared_up,
    shared_down,
    expert_ids,
    expert_weights,
):
    seq_dev, model_width = tokens.shape
    pair = lax.axis_size("tp") == 2 and model_width % 256 == 0 and seq_dev <= 8
    attend = attend_kernel if pair else attend_plain
    attn_part = attend(
        tokens,
        attn_gain,
        query_weight,
        key_weight,
        value_weight,
        out_weight,
        lambdas,
        head_gain,
        cache_keys,
        cache_values,
        lengths,
    )
    if pair:
        return routed_pair(
            tokens,
            attn_part,
            moe_gain,
            gate_weight,
            up_weight,
            down_weight,
            shared_gate,
            shared_up,
            shared_down,
            expert_ids,
            expert_weights,
        )
    attn_total = lax.psum(attn_part, "tp").astype(jnp.float32)
    mixed_rows = (tokens.astype(jnp.float32) + attn_total).astype(jnp.bfloat16)
    moe_normed = rms_scale(mixed_rows, moe_gain).astype(jnp.bfloat16)
    shared_gate_out = jnp.dot(moe_normed, shared_gate, preferred_element_type=jnp.float32)
    shared_up_out = jnp.dot(moe_normed, shared_up, preferred_element_type=jnp.float32)
    shared_hidden = (jax.nn.silu(shared_gate_out) * shared_up_out).astype(jnp.bfloat16)
    shared_part = jnp.dot(shared_hidden, shared_down, preferred_element_type=jnp.float32)
    experts = lax.axis_size("ep")
    top_count = expert_ids.shape[1]
    capacity = min(seq_dev, max(2, 2 * seq_dev * top_count // experts))
    slot_count = seq_dev * top_count
    slot_ids = expert_ids.reshape(slot_count)
    expert_hits = (slot_ids[:, None] == jnp.arange(experts, dtype=jnp.int32)[None, :]).astype(
        jnp.int32
    )
    slot_rank = jnp.sum((jnp.cumsum(expert_hits, axis=0) - expert_hits) * expert_hits, axis=1)
    slot_place = slot_ids * capacity + slot_rank
    placed = (
        slot_place[:, None] == jnp.arange(experts * capacity, dtype=jnp.int32)[None, :]
    ).astype(jnp.bfloat16)
    slot_token = jnp.arange(slot_count, dtype=jnp.int32) // top_count
    token_pick = (slot_token[:, None] == jnp.arange(seq_dev, dtype=jnp.int32)[None, :]).astype(
        jnp.bfloat16
    )
    dispatch = lax.dot_general(
        placed, token_pick, (((0,), (0,)), ((), ())), preferred_element_type=jnp.float32
    ).astype(jnp.bfloat16)
    col_count = model_width // lax.axis_size("tp")
    own_start = lax.axis_index("tp") * col_count
    own_normed = lax.dynamic_slice_in_dim(moe_normed, own_start, col_count, 1)
    send_slice = jnp.dot(dispatch, own_normed, preferred_element_type=jnp.float32).astype(
        jnp.bfloat16
    )
    arrived = lax.all_to_all(send_slice, "ep", split_axis=0, concat_axis=0, tiled=True)
    received = lax.all_gather(arrived, "tp", axis=1, tiled=True)
    gate_out = jnp.dot(received, gate_weight[0], preferred_element_type=jnp.float32)
    up_out = jnp.dot(received, up_weight[0], preferred_element_type=jnp.float32)
    expert_hidden = (jax.nn.silu(gate_out) * up_out).astype(jnp.bfloat16)
    expert_part = jnp.dot(expert_hidden, down_weight[0], preferred_element_type=jnp.float32)
    expert_sum, shared_out = scatter_sum(expert_part), scatter_sum(shared_part)
    returned = lax.all_to_all(
        expert_sum.astype(jnp.bfloat16), "ep", split_axis=0, concat_axis=0, tiled=True
    )
    slot_values = jnp.dot(placed, returned, preferred_element_type=jnp.float32).reshape(
        seq_dev, top_count, col_count
    )
    routed = jnp.sum(expert_weights[:, :, None] * slot_values, axis=1)
    own_cols = lax.dynamic_slice_in_dim(mixed_rows, own_start, col_count, 1)
    return (own_cols.astype(jnp.float32) + routed + shared_out).astype(jnp.bfloat16)


def solution(mesh):
    in_specs = (
        P("ep", None),
        P(),
        P(None, "tp"),
        P(None, "tp"),
        P(None, "tp"),
        P(None, "tp"),
        P("tp"),
        P(),
        P("ep", None, "tp", None),
        P("ep", None, "tp", None),
        P("ep"),
        P(),
        P("ep", None, "tp"),
        P("ep", None, "tp"),
        P("ep", "tp", None),
        P(None, "tp"),
        P(None, "tp"),
        P("tp", None),
        P("ep", None),
        P("ep", None),
    )
    out_specs = P("ep", "tp")
    return jax.shard_map(shards, mesh=mesh, in_specs=in_specs, out_specs=out_specs, check_vma=False)
```

profile of v0, /device:TPU:0, one launch (start us, length us, event | category | flops | bytes accessed | tf_op | source)
XLA Modules:
  0.0 57.9 jit_solution(16956987543984526071)
XLA Ops:
  0.0 0.0 copy-start
  0.0 0.0 copy-start.6
  0.0 0.0 copy-start.1
  0.0 0.0 copy-start.3
  0.0 0.0 copy-start.4
  0.0 17.0 %attend.1.own_part = bf16[7,2304]{1,0:T(8,128)(2,1)} custom-call(s32[7]{0:T(128)} %lengths_hbm.1, f32[8]{0:T(128)} %lambdas_hbm.1, bf16[7,2304]{1,0:T(8,128)(2,1)} %tokens.1, bf16[2304]{0:T(1024)(128)(2,1)} %attn_gain_hbm.1, bf16[1,128]{1,0:T(2,128)(2,1)} %bitcast.17, bf16[2304,1024]{1,0:T(8,128)(2,1)} %query_hbm.1, bf16[2304,1024]{1,0:T(8,128)(2,1)} %key_hbm.1, ...), custom_call_target="tpu_custom_call" | custom-call | tf_op jit(solution)/shard_map/attend/pallas_call | solution.py:298
  17.0 0.6 collective-permute-start
  17.6 0.0 copy-done.6
  17.6 1.1 %collective-permute-done.other_part = bf16[7,2304]{1,0:T(8,128)(2,1)S(1)} collective-permute-done((bf16[7,2304]{1,0:T(8,128)(2,1)}, bf16[7,2304]{1,0:T(8,128)(2,1)S(1)}, u32[]{:S(2)}, u32[]{:S(2)}) %collective-permute-start) | collective-permute-done | bytes 32288 | tf_op jit(solution)/shard_map/ppermute | solution.py:536
  18.7 0.0 copy-done.1
  18.7 0.0 copy-done.3
  18.7 0.0 copy-start.2
  18.7 0.8 %copy-done.2 = bf16[7,2304]{1,0:T(8,128)(2,1)S(1)} copy-done((bf16[7,2304]{1,0:T(8,128)(2,1)S(1)}, bf16[7,2304]{1,0:T(8,128)(2,1)}, u32[]{:S(2)}) %copy-start.2) | copy-done | bytes 32280
  19.5 1.2 %prepare.1 = (bf16[7,2304]{1,0:T(8,128)(2,1)S(1)}, bf16[7,2304]{1,0:T(8,128)(2,1)S(1)}, bf16[16,48,128]{2,1,0:T(8,128)(2,1)}) custom-call(s32[1]{0:T(128)} %bitcast.index, bf16[7,2304]{1,0:T(8,128)(2,1)S(1)} %copy-done.1, bf16[7,2304]{1,0:T(8,128)(2,1)S(1)} %copy-done.2, bf16[7,2304]{1,0:T(8,128)(2,1)S(1)} %collective-permute-done.other_part, ...), custom_call_target="tpu_custom_call" | custom-call | tf_op jit(solution)/shard_map/prepare/pallas_call | solution.py:540
  20.7 6.6 %all-to-all-start = ((bf16[16,48,128]{2,1,0:T(8,128)(2,1)}), bf16[16,48,128]{2,1,0:T(8,128)(2,1)S(1)}, u32[]{:S(2)}, u32[]{:S(2)}) async-start(bf16[16,48,128]{2,1,0:T(8,128)(2,1)} %get-tuple-element.14), calls=%async_computation | async-start | bytes 393216 | tf_op jit(solution)/shard_map/all_to_all | solution.py:548
  27.2 0.0 copy-done.4
  27.2 0.4 shares.1
  27.6 8.6 %all-to-all-done.own = bf16[16,48,128]{2,1,0:T(8,128)(2,1)S(1)} async-done(((bf16[16,48,128]{2,1,0:T(8,128)(2,1)}), bf16[16,48,128]{2,1,0:T(8,128)(2,1)S(1)}, u32[]{:S(2)}, u32[]{:S(2)}) %all-to-all-start) | async-done | bytes 196640 | tf_op jit(solution)/shard_map/all_to_all | solution.py:548
  36.2 0.0 collective-permute-start.1
  36.2 1.4 %collective-permute-done.1.other = bf16[16,48,128]{2,1,0:T(8,128)(2,1)S(1)} collective-permute-done((bf16[16,48,128]{2,1,0:T(8,128)(2,1)S(1)}, bf16[16,48,128]{2,1,0:T(8,128)(2,1)S(1)}, u32[]{:S(2)}, u32[]{:S(2)}) %collective-permute-start.1) | collective-permute-done | bytes 196640 | tf_op jit(solution)/shard_map/ppermute | solution.py:563
  37.6 0.0 copy-start.5
  37.6 4.5 %expert.1 = (bf16[16,48,128]{2,1,0:T(8,128)(2,1)S(1)}, bf16[16,48,128]{2,1,0:T(8,128)(2,1)S(1)}) custom-call(s32[1]{0:T(128)} %bitcast.index, bf16[16,48,128]{2,1,0:T(8,128)(2,1)S(1)} %all-to-all-done.own, bf16[16,48,128]{2,1,0:T(8,128)(2,1)S(1)} %collective-permute-done.1.other, bf16[2304,512]{1,0:T(8,128)(2,1)} %bitcast.14, bf16[2304,512]{1,0:T(8,128)(2,1)} %bitcast.15, ...), custom_call_target="tpu_custom_call" | custom-call | tf_op jit(solution)/shard_map/expert/pallas_call | solution.py:564
  42.1 0.2 collective-permute-start.2
  42.3 0.0 copy-done.5
  42.3 0.4 fusion.4
  42.7 0.9 %collective-permute-done.2 = bf16[16,48,128]{2,1,0:T(8,128)(2,1)S(1)} collective-permute-done((bf16[16,48,128]{2,1,0:T(8,128)(2,1)S(1)}, bf16[16,48,128]{2,1,0:T(8,128)(2,1)S(1)}, u32[]{:S(2)}, u32[]{:S(2)}) %collective-permute-start.2) | collective-permute-done | bytes 196640 | tf_op jit(solution)/shard_map/ppermute | solution.py:587
  43.6 0.7 %add_convert_fusion = bf16[16,48,128]{2,1,0:T(8,128)(2,1)} fusion(bf16[16,48,128]{2,1,0:T(8,128)(2,1)S(1)} %collective-permute-done.2, bf16[16,48,128]{2,1,0:T(8,128)(2,1)S(1)} %get-tuple-element.18), kind=kLoop, calls=%fused_computation.1 | loop fusion | flops 393216 | bytes 589824 | tf_op jit(solution)/shard_map/convert_element_type | solution.py:589
  44.4 3.5 %all-to-all-start.1 = ((bf16[16,48,128]{2,1,0:T(8,128)(2,1)}), bf16[16,48,128]{2,1,0:T(8,128)(2,1)S(1)}, u32[]{:S(2)}, u32[]{:S(2)}) async-start(bf16[16,48,128]{2,1,0:T(8,128)(2,1)} %add_convert_fusion), calls=%async_computation.1 | async-start | bytes 393216 | tf_op jit(solution)/shard_map/all_to_all | solution.py:588
  47.9 0.0 copy-done
  47.9 2.5 %convolution_convert_fusion.own_shared = bf16[7,2304]{1,0:T(8,128)(2,1)S(1)} fusion(bf16[512,2304]{1,0:T(8,128)(2,1)S(1)} %copy-done, f32[7,512]{1,0:T(8,128)S(1)} %fusion.4, bf16[7,2304]{1,0:T(8,128)(2,1)S(1)} %get-tuple-element.15.after, bf16[2304,512]{1,0:T(8,128)(2,1)} %param.36), kind=kOutput, calls=%fused_computation | convolution fusion | flops 33067776 | bytes 4797440 | tf_op jit(solution)/shard_map/dot_general | solution.py:594
  50.4 0.2 collective-permute-start.3
  50.5 1.1 %collective-permute-done.3.other_shared = bf16[7,1152]{1,0:T(8,128)(2,1)S(1)} collective-permute-done((bf16[7,1152]{1,0:T(8,128)(2,1)S(1)}, bf16[7,1152]{1,0:T(8,128)(2,1)S(1)}, u32[]{:S(2)}, u32[]{:S(2)}) %collective-permute-start.3) | collective-permute-done | bytes 16160 | tf_op jit(solution)/shard_map/ppermute | solution.py:597
  51.6 5.2 %all-to-all-done.1.returned = bf16[16,48,128]{2,1,0:T(8,128)(2,1)S(1)} async-done(((bf16[16,48,128]{2,1,0:T(8,128)(2,1)}), bf16[16,48,128]{2,1,0:T(8,128)(2,1)S(1)}, u32[]{:S(2)}, u32[]{:S(2)}) %all-to-all-start.1) | async-done | bytes 196640 | tf_op jit(solution)/shard_map/all_to_all | solution.py:588
  56.8 1.1 %combine.1 = bf16[7,1152]{1,0:T(8,128)(2,1)} custom-call(s32[1]{0:T(128)} %bitcast.index, bf16[16,48,128]{2,1,0:T(8,128)(2,1)S(1)} %all-to-all-done.1.returned, bf16[16,72,48]{2,1,0:T(8,128)(2,1)S(1)} %get-tuple-element.20.high, bf16[16,72,48]{2,1,0:T(8,128)(2,1)S(1)} %get-tuple-element.21.low, bf16[7,2304]{1,0:T(8,128)(2,1)S(1)} %get-tuple-element.22.mixed, ...), custom_call_target="tpu_custom_call" | custom-call | tf_op jit(solution)/shard_map/combine/pallas_call | solution.py:598
  (2 shorter events, 0.0 us)
Async XLA Ops:
  0.0 47.9 %copy-start = (bf16[512,2304]{1,0:T(8,128)(2,1)S(1)}, bf16[512,2304]{1,0:T(8,128)(2,1)}, u32[]{:S(2)}) copy-start(bf16[512,2304]{1,0:T(8,128)(2,1)} %param.37) | copy-start | bytes 7077892
  0.0 17.6 %copy-start.6 = (bf16[2304]{0:T(1024)(128)(2,1)S(1)}, bf16[2304]{0:T(1024)(128)(2,1)}, u32[]{:S(2)}) copy-start(bf16[2304]{0:T(1024)(128)(2,1)} %param.31) | copy-start | bytes 13828
  0.0 18.7 %copy-start.1 = (bf16[7,2304]{1,0:T(8,128)(2,1)S(1)}, bf16[7,2304]{1,0:T(8,128)(2,1)}, u32[]{:S(2)}) copy-start(bf16[7,2304]{1,0:T(8,128)(2,1)} %tokens.1) | copy-start | bytes 96772
  0.0 18.7 %copy-start.3 = (s32[7,6]{1,0:T(8,128)S(1)}, s32[7,6]{1,0:T(8,128)}, u32[]{:S(2)}) copy-start(s32[7,6]{1,0:T(8,128)} %ids.3) | copy-start | bytes 508
  0.0 27.2 %copy-start.4 = (f32[7,6]{1,0:T(8,128)S(1)}, f32[7,6]{1,0:T(8,128)}, u32[]{:S(2)}) copy-start(f32[7,6]{1,0:T(8,128)} %weights.1) | copy-start | bytes 508
  17.0 1.6 %collective-permute-start = (bf16[7,2304]{1,0:T(8,128)(2,1)}, bf16[7,2304]{1,0:T(8,128)(2,1)S(1)}, u32[]{:S(2)}, u32[]{:S(2)}) collective-permute-start(bf16[7,2304]{1,0:T(8,128)(2,1)} %attend.1.own_part), channel_id=1, source_target_pairs={{0,1},{1,0},{2,3},{3,2},{4,5},{5,4},{6,7},{7,6},{8,9},{9,8},{10,11... | collective-permute-start | bytes 96776 | tf_op jit(solution)/shard_map/ppermute | solution.py:536
  18.7 0.8 %copy-start.2 = (bf16[7,2304]{1,0:T(8,128)(2,1)S(1)}, bf16[7,2304]{1,0:T(8,128)(2,1)}, u32[]{:S(2)}) copy-start(bf16[7,2304]{1,0:T(8,128)(2,1)} %attend.1.own_part) | copy-start | bytes 96772
  20.7 15.5 %all-to-all-start = ((bf16[16,48,128]{2,1,0:T(8,128)(2,1)}), bf16[16,48,128]{2,1,0:T(8,128)(2,1)S(1)}, u32[]{:S(2)}, u32[]{:S(2)}) async-start(bf16[16,48,128]{2,1,0:T(8,128)(2,1)} %get-tuple-element.14), calls=%async_computation | async-start | bytes 393216 | tf_op jit(solution)/shard_map/all_to_all | solution.py:548
  36.2 1.4 %collective-permute-start.1 = (bf16[16,48,128]{2,1,0:T(8,128)(2,1)S(1)}, bf16[16,48,128]{2,1,0:T(8,128)(2,1)S(1)}, u32[]{:S(2)}, u32[]{:S(2)}) collective-permute-start(bf16[16,48,128]{2,1,0:T(8,128)(2,1)S(1)} %all-to-all-done.own), channel_id=1, source_target_pairs={{0,1},{1,0},{2,3},{3,2},{4,5},{5,4},{6,7},{7,6},{8,9},{9,8},{10,11... | collective-permute-start | bytes 589832 | tf_op jit(solution)/shard_map/ppermute | solution.py:563
  37.6 4.7 %copy-start.5 = (bf16[2304,512]{1,0:T(8,128)(2,1)S(1)}, bf16[2304,512]{1,0:T(8,128)(2,1)}, u32[]{:S(2)}) copy-start(bf16[2304,512]{1,0:T(8,128)(2,1)} %param.35) | copy-start | bytes 7077892
  42.1 1.5 %collective-permute-start.2 = (bf16[16,48,128]{2,1,0:T(8,128)(2,1)S(1)}, bf16[16,48,128]{2,1,0:T(8,128)(2,1)S(1)}, u32[]{:S(2)}, u32[]{:S(2)}) collective-permute-start(bf16[16,48,128]{2,1,0:T(8,128)(2,1)S(1)} %get-tuple-element.19), channel_id=1, source_target_pairs={{0,1},{1,0},{2,3},{3,2},{4,5},{5,4},{6,7},{7,6},{8,9},{9,8},{10,11... | collective-permute-start | bytes 589832 | tf_op jit(solution)/shard_map/ppermute | solution.py:587
  44.4 12.4 %all-to-all-start.1 = ((bf16[16,48,128]{2,1,0:T(8,128)(2,1)}), bf16[16,48,128]{2,1,0:T(8,128)(2,1)S(1)}, u32[]{:S(2)}, u32[]{:S(2)}) async-start(bf16[16,48,128]{2,1,0:T(8,128)(2,1)} %add_convert_fusion), calls=%async_computation.1 | async-start | bytes 393216 | tf_op jit(solution)/shard_map/all_to_all | solution.py:588
  50.4 1.2 %collective-permute-start.3 = (bf16[7,1152]{1,0:T(8,128)(2,1)S(1)}, bf16[7,1152]{1,0:T(8,128)(2,1)S(1)}, u32[]{:S(2)}, u32[]{:S(2)}) collective-permute-start(bf16[7,1152]{1,0:T(8,128)(2,1)S(1)} %constant_dynamic-slice_fusion), channel_id=1, source_target_pairs={{0,1},{1,0},{2,3},{3,2},{4,5},{5,4},{6,7},{7,6},{8,9},{9,8},{10,11... | collective-permute-start | bytes 48392 | tf_op jit(solution)/shard_map/ppermute | solution.py:597
where the time goes:
time: 58.5 us; the launch traced here: 57.9 us
  Pallas kernels  24.2 us (41%)
  waiting for transfers between devices  18.2 us (31%)
  starting transfers between devices  11 us (19%)
  matrix products  2.89 us (5%)
  local copies, waits for them, and re-layouts  0.8 us (1%)
  other arithmetic  0.72 us (1%)
    pallas_call x1, Pallas kernels, attend_kernel(): pl.pallas_call(attend_body, out_shape=jax.ShapeDtypeStruct((seq_dev, mode...  17 us
    all_to_all x1, waiting for transfers between devices, routed_pair(): lax.all_to_all(send, 'ep', split_axis=0, concat_axis=0, tiled=True)  8.56 us
    all_to_all x1, starting transfers between devices, routed_pair(): lax.all_to_all(send, 'ep', split_axis=0, concat_axis=0, tiled=True)  6.57 us
    all_to_all x1, waiting for transfers between devices, routed_pair(): lax.all_to_all(expert_sum.astype(bf16), 'ep', split_axis=0, concat_axis=0...  5.17 us
    pallas_call x1, Pallas kernels, routed_pair(): pl.pallas_call(expert_body, out_shape=(packed, packed), in_specs=[smem] +...  4.48 us
    all_to_all x1, starting transfers between devices, routed_pair(): lax.all_to_all(expert_sum.astype(bf16), 'ep', split_axis=0, concat_axis=0...  3.52 us
    dot_general x1, matrix products, routed_pair(): jnp.dot(shared_hidden, shared_down, preferred_element_type=jnp.float32)  2.49 us
    ppermute x1, waiting for transfers between devices, routed_pair(): partner = lax.ppermute(arrived, 'tp', swap)  1.44 us
  transfers between devices with their start and end apart: 6, of which 6 were waited for; matrix products, arithmetic and copies ran while one was open for 5% of the time, Pallas kernels for 1%

commit v1 on v0

--- a/solution.py
+++ b/solution.py
@@ -7,6 +7,7 @@
 
 epsilon = 1e-06
 GRAIN = 128
+STEP = 256
 CHUNK = 1024
 PIECES = 1
 FLIGHT = 3
@@ -122,7 +123,7 @@
             values[s, rows, :] = jnp.zeros((grain_rows, width), jnp.bfloat16)
             return carry
 
-        used = jnp.where(lengths[s] > cache_rows // heads // 2, cache_rows, cache_rows // 2)
+        used = (lengths[s] + STEP - 1) // STEP * STEP * heads
         return lax.fori_loop(live_rows(s) // grain_rows, used // grain_rows, clear, carry)
 
     lax.fori_loop(0, seq_dev, clear_tail, 0)
@@ -227,12 +228,12 @@
         head_outs[s] = acc[:heads, :width] + acc[heads:, width:] + own_mixture * new_values[s]
 
     full = cache_rows // heads
-    sizes = (full // 2, full)
+    sizes = tuple(range(STEP, full + 1, STEP))
 
     def sized(run, s):
         for size in sizes:
 
-            @pl.when((lengths[s] > sizes[0]) == (size == full))
+            @pl.when((lengths[s] > size - STEP) & (lengths[s] <= size))
             def _():
                 run(s, size)
 
@@ -378,16 +379,15 @@
     return jnp.concatenate([rows, jnp.full((8 - seq_dev, cols), value, rows.dtype)], axis=0)
 
 
-def prepare_body(index, tokens, own_part, other_part, gain, ids, mixed_out, normed_out, send_out):
+def prepare_body(
+    index, tokens, own_hbm, other_part, gain, ids, mixed_out, normed_out, send_out, own_part, sem
+):
+    copy = pltpu.make_async_copy(own_hbm, own_part, sem)
+    copy.start()
     experts, block, lanes = send_out.shape
     cols = tokens.shape[1] // 2
     chunks = cols // lanes
     cap = capacity_of(tokens.shape[0], ids.shape[1], experts)
-    total = own_part[...].astype(jnp.float32) + other_part[...].astype(jnp.float32)
-    mixed = (tokens[...].astype(jnp.float32) + total).astype(jnp.bfloat16)
-    mixed_out[...] = mixed
-    normed = rms_scale(mixed, gain[...]).astype(jnp.bfloat16)
-    normed_out[...] = normed
     codes = padded_rows(slot_codes(ids[...], experts), -1.0)
     codes = jnp.concatenate([codes] * chunks, axis=0)
     expert = lax.broadcasted_iota(jnp.int32, (experts, experts), 0)
@@ -401,6 +401,12 @@
     rank, _ = slot_map((block, chunks * 8), cap, 0, 1)
     picks = [jnp.where(code_rows[e : e + 1, :] == rank, 1.0, 0.0) for e in range(experts)]
     picks = jnp.concatenate(picks, axis=0).astype(jnp.bfloat16)
+    copy.wait()
+    total = own_part[...].astype(jnp.float32) + other_part[...].astype(jnp.float32)
+    mixed = (tokens[...].astype(jnp.float32) + total).astype(jnp.bfloat16)
+    mixed_out[...] = mixed
+    normed = rms_scale(mixed, gain[...]).astype(jnp.bfloat16)
+    normed_out[...] = normed
     wide = padded_rows(normed.astype(jnp.float32), 0.0)
     low = index[0] == 0
     stack = [
@@ -440,8 +446,8 @@
 ):
     pairs = ((gate_hbm, gate), (up_hbm, up), (down_hbm, down))
     copies = [pltpu.make_async_copy(a, b, sems.at[i]) for i, (a, b) in enumerate(pairs)]
-    for copy in copies:
-        copy.start()
+    copies[0].start()
+    copies[1].start()
     experts, block, lanes = own.shape
     cols = rows.shape[1] // 2
     chunks = cols // lanes
@@ -458,6 +464,7 @@
             for c in range(chunks):
                 at = pl.ds(pl.multiple_of(start + c * lanes, lanes), lanes)
                 rows[e * 8 : (e + 1) * 8, at] = got[c * 8 : (c + 1) * 8]
+    copies[2].start()
     x = rows[...].astype(jnp.bfloat16)
     copies[0].wait()
     gate_part = jnp.dot(x, gate[...], preferred_element_type=jnp.float32)
@@ -540,8 +547,9 @@
     mixed, normed, send = pl.pallas_call(
         prepare_body,
         out_shape=(rows, rows, packed),
-        in_specs=[smem] + [vmem] * 5,
+        in_specs=[smem, vmem, anywhere] + [vmem] * 3,
         out_specs=(vmem,) * 3,
+        scratch_shapes=[pltpu.VMEM((seq_dev, model_width), bf16), pltpu.SemaphoreType.DMA],
         compiler_params=pltpu.CompilerParams(vmem_limit_bytes=8 << 20),
         name="prepare",
     )(index, tokens, attn_part, other_part, moe_gain.reshape(1, -1), expert_ids)
@@ -705,7 +713,9 @@
     expert_weights,
 ):
     seq_dev, model_width = tokens.shape
+    cache_len, local_heads = cache_keys.shape[1:3]
     pair = lax.axis_size("tp") == 2 and model_width % 256 == 0 and seq_dev <= 8
+    pair = pair and cache_len % STEP == 0 and STEP * local_heads % (2 * CHUNK) == 0
     attend = attend_kernel if pair else attend_plain
     attn_part = attend(
         tokens,

time: 58.5 us -> 57.5 us (0.983)
  Pallas kernels: 24.2 us -> 21.8 us
  starting transfers between devices: 11 us -> 12.3 us
    pallas_call x1, Pallas kernels: 17 us -> 14.4 us  [attend_kernel(): pl.pallas_call(attend_body, out_shape=jax.ShapeDtypeStruct((seq_dev, mode...]
    all_to_all x1, starting transfers between devices: 6.57 us -> 7.85 us  [routed_pair(): lax.all_to_all(send, 'ep', split_axis=0, concat_axis=0, tiled=True)]
where the time goes in v1:
time: 57.5 us; the launch traced here: 56.8 us
  Pallas kernels  21.8 us (38%)
  waiting for transfers between devices  18.2 us (32%)
  starting transfers between devices  12.3 us (21%)
  matrix products  2.89 us (5%)
  local copies, waits for them, and re-layouts  0.8 us (1%)
  other arithmetic  0.72 us (1%)
    pallas_call x1, Pallas kernels, attend_kernel(): pl.pallas_call(attend_body, out_shape=jax.ShapeDtypeStruct((seq_dev, mode...  14.4 us
    all_to_all x1, waiting for transfers between devices, routed_pair(): lax.all_to_all(send, 'ep', split_axis=0, concat_axis=0, tiled=True)  8.56 us
    all_to_all x1, starting transfers between devices, routed_pair(): lax.all_to_all(send, 'ep', split_axis=0, concat_axis=0, tiled=True)  7.85 us
    all_to_all x1, waiting for transfers between devices, routed_pair(): lax.all_to_all(expert_sum.astype(bf16), 'ep', split_axis=0, concat_axis=0...  5.17 us
    pallas_call x1, Pallas kernels, routed_pair(): pl.pallas_call(expert_body, out_shape=(packed, packed), in_specs=[smem] +...  4.49 us
    all_to_all x1, starting transfers between devices, routed_pair(): lax.all_to_all(expert_sum.astype(bf16), 'ep', split_axis=0, concat_axis=0...  3.52 us
    dot_general x1, matrix products, routed_pair(): jnp.dot(shared_hidden, shared_down, preferred_element_type=jnp.float32)  2.49 us
    ppermute x1, waiting for transfers between devices, routed_pair(): partner = lax.ppermute(arrived, 'tp', swap)  1.44 us
  transfers between devices with their start and end apart: 6, of which 6 were waited for; matrix products, arithmetic and copies ran while one was open for 5% of the time, Pallas kernels for 1%

profile of v1, /device:TPU:0, one launch (start us, length us, event | category | flops | bytes accessed | tf_op | source)
XLA Modules:
  0.0 56.8 jit_solution(9603063309320187687)
XLA Ops:
  0.0 0.0 copy-start
  0.0 0.0 copy-start.6
  0.0 0.0 copy-start.1
  0.0 0.0 copy-start.3
  0.0 0.0 copy-start.4
  0.0 14.4 %attend.1.own_hbm = bf16[7,2304]{1,0:T(8,128)(2,1)} custom-call(s32[7]{0:T(128)} %lengths_hbm.1, f32[8]{0:T(128)} %lambdas_hbm.1, bf16[7,2304]{1,0:T(8,128)(2,1)} %tokens.1, bf16[2304]{0:T(1024)(128)(2,1)} %attn_gain_hbm.1, bf16[1,128]{1,0:T(2,128)(2,1)} %bitcast.17, bf16[2304,1024]{1,0:T(8,128)(2,1)} %query_hbm.1, bf16[2304,1024]{1,0:T(8,128)(2,1)} %key_hbm.1, ...), custom_call_target="tpu_custom_call" | custom-call | tf_op jit(solution)/shard_map/attend/pallas_call | solution.py:299
  14.5 0.6 collective-permute-start
  15.0 0.0 copy-done.6
  15.0 1.1 %collective-permute-done.other_part = bf16[7,2304]{1,0:T(8,128)(2,1)S(1)} collective-permute-done((bf16[7,2304]{1,0:T(8,128)(2,1)}, bf16[7,2304]{1,0:T(8,128)(2,1)S(1)}, u32[]{:S(2)}, u32[]{:S(2)}) %collective-permute-start) | collective-permute-done | bytes 32288 | tf_op jit(solution)/shard_map/ppermute | solution.py:543
  16.1 0.0 copy-done.1
  16.1 0.0 copy-done.3
  16.1 0.0 copy-start.2
  16.1 0.8 %copy-done.2 = bf16[7,2304]{1,0:T(8,128)(2,1)S(1)} copy-done((bf16[7,2304]{1,0:T(8,128)(2,1)S(1)}, bf16[7,2304]{1,0:T(8,128)(2,1)}, u32[]{:S(2)}) %copy-start.2) | copy-done | bytes 32280
  16.9 1.4 %prepare.1 = (bf16[7,2304]{1,0:T(8,128)(2,1)S(1)}, bf16[7,2304]{1,0:T(8,128)(2,1)S(1)}, bf16[16,48,128]{2,1,0:T(8,128)(2,1)}) custom-call(s32[1]{0:T(128)} %bitcast.index, bf16[7,2304]{1,0:T(8,128)(2,1)S(1)} %copy-done.1, bf16[7,2304]{1,0:T(8,128)(2,1)S(1)} %copy-done.2, bf16[7,2304]{1,0:T(8,128)(2,1)S(1)} %collective-permute-done.other_part, ...), custom_call_target="tpu_custom_call" | custom-call | tf_op jit(solution)/shard_map/prepare/pallas_call | solution.py:547
  18.3 7.9 %all-to-all-start = ((bf16[16,48,128]{2,1,0:T(8,128)(2,1)}), bf16[16,48,128]{2,1,0:T(8,128)(2,1)S(1)}, u32[]{:S(2)}, u32[]{:S(2)}) async-start(bf16[16,48,128]{2,1,0:T(8,128)(2,1)} %get-tuple-element.14), calls=%async_computation | async-start | bytes 393216 | tf_op jit(solution)/shard_map/all_to_all | solution.py:556
  26.1 0.0 copy-done.4
  26.1 0.4 shares.1
  26.5 8.6 %all-to-all-done.own = bf16[16,48,128]{2,1,0:T(8,128)(2,1)S(1)} async-done(((bf16[16,48,128]{2,1,0:T(8,128)(2,1)}), bf16[16,48,128]{2,1,0:T(8,128)(2,1)S(1)}, u32[]{:S(2)}, u32[]{:S(2)}) %all-to-all-start) | async-done | bytes 196640 | tf_op jit(solution)/shard_map/all_to_all | solution.py:556
  35.1 0.0 collective-permute-start.1
  35.1 1.4 %collective-permute-done.1.other = bf16[16,48,128]{2,1,0:T(8,128)(2,1)S(1)} collective-permute-done((bf16[16,48,128]{2,1,0:T(8,128)(2,1)S(1)}, bf16[16,48,128]{2,1,0:T(8,128)(2,1)S(1)}, u32[]{:S(2)}, u32[]{:S(2)}) %collective-permute-start.1) | collective-permute-done | bytes 196640 | tf_op jit(solution)/shard_map/ppermute | solution.py:571
  36.5 0.0 copy-start.5
  36.5 4.5 %expert.1 = (bf16[16,48,128]{2,1,0:T(8,128)(2,1)S(1)}, bf16[16,48,128]{2,1,0:T(8,128)(2,1)S(1)}) custom-call(s32[1]{0:T(128)} %bitcast.index, bf16[16,48,128]{2,1,0:T(8,128)(2,1)S(1)} %all-to-all-done.own, bf16[16,48,128]{2,1,0:T(8,128)(2,1)S(1)} %collective-permute-done.1.other, bf16[2304,512]{1,0:T(8,128)(2,1)} %bitcast.14, bf16[2304,512]{1,0:T(8,128)(2,1)} %bitcast.15, ...), custom_call_target="tpu_custom_call" | custom-call | tf_op jit(solution)/shard_map/expert/pallas_call | solution.py:572
  41.0 0.2 collective-permute-start.2
  41.2 0.0 copy-done.5
  41.2 0.4 fusion.4
  41.6 0.9 %collective-permute-done.2 = bf16[16,48,128]{2,1,0:T(8,128)(2,1)S(1)} collective-permute-done((bf16[16,48,128]{2,1,0:T(8,128)(2,1)S(1)}, bf16[16,48,128]{2,1,0:T(8,128)(2,1)S(1)}, u32[]{:S(2)}, u32[]{:S(2)}) %collective-permute-start.2) | collective-permute-done | bytes 196640 | tf_op jit(solution)/shard_map/ppermute | solution.py:595
  42.5 0.7 %add_convert_fusion = bf16[16,48,128]{2,1,0:T(8,128)(2,1)} fusion(bf16[16,48,128]{2,1,0:T(8,128)(2,1)S(1)} %collective-permute-done.2, bf16[16,48,128]{2,1,0:T(8,128)(2,1)S(1)} %get-tuple-element.18), kind=kLoop, calls=%fused_computation.1 | loop fusion | flops 393216 | bytes 589824 | tf_op jit(solution)/shard_map/convert_element_type | solution.py:597
  43.3 3.5 %all-to-all-start.1 = ((bf16[16,48,128]{2,1,0:T(8,128)(2,1)}), bf16[16,48,128]{2,1,0:T(8,128)(2,1)S(1)}, u32[]{:S(2)}, u32[]{:S(2)}) async-start(bf16[16,48,128]{2,1,0:T(8,128)(2,1)} %add_convert_fusion), calls=%async_computation.1 | async-start | bytes 393216 | tf_op jit(solution)/shard_map/all_to_all | solution.py:596
  46.8 0.0 copy-done
  46.8 2.5 %convolution_convert_fusion.own_shared = bf16[7,2304]{1,0:T(8,128)(2,1)S(1)} fusion(bf16[512,2304]{1,0:T(8,128)(2,1)S(1)} %copy-done, f32[7,512]{1,0:T(8,128)S(1)} %fusion.4, bf16[7,2304]{1,0:T(8,128)(2,1)S(1)} %get-tuple-element.15.after, bf16[2304,512]{1,0:T(8,128)(2,1)} %param.36), kind=kOutput, calls=%fused_computation | convolution fusion | flops 33067776 | bytes 4797440 | tf_op jit(solution)/shard_map/dot_general | solution.py:602
  49.3 0.2 collective-permute-start.3
  49.5 1.1 %collective-permute-done.3.other_shared = bf16[7,1152]{1,0:T(8,128)(2,1)S(1)} collective-permute-done((bf16[7,1152]{1,0:T(8,128)(2,1)S(1)}, bf16[7,1152]{1,0:T(8,128)(2,1)S(1)}, u32[]{:S(2)}, u32[]{:S(2)}) %collective-permute-start.3) | collective-permute-done | bytes 16160 | tf_op jit(solution)/shard_map/ppermute | solution.py:605
  50.5 5.2 %all-to-all-done.1.returned = bf16[16,48,128]{2,1,0:T(8,128)(2,1)S(1)} async-done(((bf16[16,48,128]{2,1,0:T(8,128)(2,1)}), bf16[16,48,128]{2,1,0:T(8,128)(2,1)S(1)}, u32[]{:S(2)}, u32[]{:S(2)}) %all-to-all-start.1) | async-done | bytes 196640 | tf_op jit(solution)/shard_map/all_to_all | solution.py:596
  55.7 1.1 %combine.1 = bf16[7,1152]{1,0:T(8,128)(2,1)} custom-call(s32[1]{0:T(128)} %bitcast.index, bf16[16,48,128]{2,1,0:T(8,128)(2,1)S(1)} %all-to-all-done.1.returned, bf16[16,72,48]{2,1,0:T(8,128)(2,1)S(1)} %get-tuple-element.20.high, bf16[16,72,48]{2,1,0:T(8,128)(2,1)S(1)} %get-tuple-element.21.low, bf16[7,2304]{1,0:T(8,128)(2,1)S(1)} %get-tuple-element.22.mixed, ...), custom_call_target="tpu_custom_call" | custom-call | tf_op jit(solution)/shard_map/combine/pallas_call | solution.py:606
  (2 shorter events, 0.0 us)
Async XLA Ops:
  0.0 46.8 %copy-start = (bf16[512,2304]{1,0:T(8,128)(2,1)S(1)}, bf16[512,2304]{1,0:T(8,128)(2,1)}, u32[]{:S(2)}) copy-start(bf16[512,2304]{1,0:T(8,128)(2,1)} %param.37) | copy-start | bytes 7077892
  0.0 15.0 %copy-start.6 = (bf16[2304]{0:T(1024)(128)(2,1)S(1)}, bf16[2304]{0:T(1024)(128)(2,1)}, u32[]{:S(2)}) copy-start(bf16[2304]{0:T(1024)(128)(2,1)} %param.31) | copy-start | bytes 13828
  0.0 16.1 %copy-start.1 = (bf16[7,2304]{1,0:T(8,128)(2,1)S(1)}, bf16[7,2304]{1,0:T(8,128)(2,1)}, u32[]{:S(2)}) copy-start(bf16[7,2304]{1,0:T(8,128)(2,1)} %tokens.1) | copy-start | bytes 96772
  0.0 16.1 %copy-start.3 = (s32[7,6]{1,0:T(8,128)S(1)}, s32[7,6]{1,0:T(8,128)}, u32[]{:S(2)}) copy-start(s32[7,6]{1,0:T(8,128)} %ids.3) | copy-start | bytes 508
  0.0 26.1 %copy-start.4 = (f32[7,6]{1,0:T(8,128)S(1)}, f32[7,6]{1,0:T(8,128)}, u32[]{:S(2)}) copy-start(f32[7,6]{1,0:T(8,128)} %weights.1) | copy-start | bytes 508
  14.5 1.6 %collective-permute-start = (bf16[7,2304]{1,0:T(8,128)(2,1)}, bf16[7,2304]{1,0:T(8,128)(2,1)S(1)}, u32[]{:S(2)}, u32[]{:S(2)}) collective-permute-start(bf16[7,2304]{1,0:T(8,128)(2,1)} %attend.1.own_hbm), channel_id=1, source_target_pairs={{0,1},{1,0},{2,3},{3,2},{4,5},{5,4},{6,7},{7,6},{8,9},{9,8},{10,11... | collective-permute-start | bytes 96776 | tf_op jit(solution)/shard_map/ppermute | solution.py:543
  16.1 0.8 %copy-start.2 = (bf16[7,2304]{1,0:T(8,128)(2,1)S(1)}, bf16[7,2304]{1,0:T(8,128)(2,1)}, u32[]{:S(2)}) copy-start(bf16[7,2304]{1,0:T(8,128)(2,1)} %attend.1.own_hbm) | copy-start | bytes 96772
  18.3 16.8 %all-to-all-start = ((bf16[16,48,128]{2,1,0:T(8,128)(2,1)}), bf16[16,48,128]{2,1,0:T(8,128)(2,1)S(1)}, u32[]{:S(2)}, u32[]{:S(2)}) async-start(bf16[16,48,128]{2,1,0:T(8,128)(2,1)} %get-tuple-element.14), calls=%async_computation | async-start | bytes 393216 | tf_op jit(solution)/shard_map/all_to_all | solution.py:556
  35.1 1.4 %collective-permute-start.1 = (bf16[16,48,128]{2,1,0:T(8,128)(2,1)S(1)}, bf16[16,48,128]{2,1,0:T(8,128)(2,1)S(1)}, u32[]{:S(2)}, u32[]{:S(2)}) collective-permute-start(bf16[16,48,128]{2,1,0:T(8,128)(2,1)S(1)} %all-to-all-done.own), channel_id=1, source_target_pairs={{0,1},{1,0},{2,3},{3,2},{4,5},{5,4},{6,7},{7,6},{8,9},{9,8},{10,11... | collective-permute-start | bytes 589832 | tf_op jit(solution)/shard_map/ppermute | solution.py:571
  36.5 4.7 %copy-start.5 = (bf16[2304,512]{1,0:T(8,128)(2,1)S(1)}, bf16[2304,512]{1,0:T(8,128)(2,1)}, u32[]{:S(2)}) copy-start(bf16[2304,512]{1,0:T(8,128)(2,1)} %param.35) | copy-start | bytes 7077892
  41.0 1.5 %collective-permute-start.2 = (bf16[16,48,128]{2,1,0:T(8,128)(2,1)S(1)}, bf16[16,48,128]{2,1,0:T(8,128)(2,1)S(1)}, u32[]{:S(2)}, u32[]{:S(2)}) collective-permute-start(bf16[16,48,128]{2,1,0:T(8,128)(2,1)S(1)} %get-tuple-element.19), channel_id=1, source_target_pairs={{0,1},{1,0},{2,3},{3,2},{4,5},{5,4},{6,7},{7,6},{8,9},{9,8},{10,11... | collective-permute-start | bytes 589832 | tf_op jit(solution)/shard_map/ppermute | solution.py:595
  43.3 12.4 %all-to-all-start.1 = ((bf16[16,48,128]{2,1,0:T(8,128)(2,1)}), bf16[16,48,128]{2,1,0:T(8,128)(2,1)S(1)}, u32[]{:S(2)}, u32[]{:S(2)}) async-start(bf16[16,48,128]{2,1,0:T(8,128)(2,1)} %add_convert_fusion), calls=%async_computation.1 | async-start | bytes 393216 | tf_op jit(solution)/shard_map/all_to_all | solution.py:596
  49.3 1.2 %collective-permute-start.3 = (bf16[7,1152]{1,0:T(8,128)(2,1)S(1)}, bf16[7,1152]{1,0:T(8,128)(2,1)S(1)}, u32[]{:S(2)}, u32[]{:S(2)}) collective-permute-start(bf16[7,1152]{1,0:T(8,128)(2,1)S(1)} %constant_dynamic-slice_fusion), channel_id=1, source_target_pairs={{0,1},{1,0},{2,3},{3,2},{4,5},{5,4},{6,7},{7,6},{8,9},{9,8},{10,11... | collective-permute-start | bytes 48392 | tf_op jit(solution)/shard_map/ppermute | solution.py:605

commit v2 on v1

--- a/solution.py
+++ b/solution.py
@@ -552,7 +552,14 @@
         scratch_shapes=[pltpu.VMEM((seq_dev, model_width), bf16), pltpu.SemaphoreType.DMA],
         compiler_params=pltpu.CompilerParams(vmem_limit_bytes=8 << 20),
         name="prepare",
-    )(index, tokens, attn_part, other_part, moe_gain.reshape(1, -1), expert_ids)
+    )(
+        index,
+        tokens,
+        pltpu.with_memory_space_constraint(attn_part, pltpu.HBM),
+        other_part,
+        moe_gain.reshape(1, -1),
+        expert_ids,
+    )
     arrived = lax.all_to_all(send, "ep", split_axis=0, concat_axis=0, tiled=True)
     hidden = gate_weight.shape[2]
     mix = shape((experts, chunks * 8, block), bf16)

time: 57.5 us -> 57.3 us (level)
  local copies, waits for them, and re-layouts: 0.8 us -> 0.04 us
    unnamed x14 -> x12, local copies, waits for them, and re-layouts: 0.79 us -> 0.02 us
where the time goes in v2:
time: 57.3 us; the launch traced here: 56.7 us
  Pallas kernels  22 us (38%)
  waiting for transfers between devices  18.2 us (32%)
  starting transfers between devices  12.8 us (22%)
  matrix products  2.89 us (5%)
  other arithmetic  0.73 us (1%)
    pallas_call x1, Pallas kernels, attend_kernel(): pl.pallas_call(attend_body, out_shape=jax.ShapeDtypeStruct((seq_dev, mode...  14.3 us
    all_to_all x1, waiting for transfers between devices, routed_pair(): lax.all_to_all(send, 'ep', split_axis=0, concat_axis=0, tiled=True)  8.57 us
    all_to_all x1, starting transfers between devices, routed_pair(): lax.all_to_all(send, 'ep', split_axis=0, concat_axis=0, tiled=True)  8.33 us
    all_to_all x1, waiting for transfers between devices, routed_pair(): lax.all_to_all(expert_sum.astype(bf16), 'ep', split_axis=0, concat_axis=0...  5.17 us
    pallas_call x1, Pallas kernels, routed_pair(): pl.pallas_call(expert_body, out_shape=(packed, packed), in_specs=[smem] +...  4.48 us
    all_to_all x1, starting transfers between devices, routed_pair(): lax.all_to_all(expert_sum.astype(bf16), 'ep', split_axis=0, concat_axis=0...  3.52 us
    dot_general x1, matrix products, routed_pair(): jnp.dot(shared_hidden, shared_down, preferred_element_type=jnp.float32)  2.49 us
    pallas_call x1, Pallas kernels, routed_pair(): pl.pallas_call(prepare_body, out_shape=(rows, rows, packed), in_specs=[sm...  1.78 us
  transfers between devices with their start and end apart: 6, of which 6 were waited for; matrix products, arithmetic and copies ran while one was open for 5% of the time, Pallas kernels for 1%

profile of v2, /device:TPU:0, one launch (start us, length us, event | category | flops | bytes accessed | tf_op | source)
XLA Modules:
  0.0 56.7 jit_solution(13184945569388906144)
XLA Ops:
  0.0 0.0 copy-start
  0.0 0.0 copy-start.5
  0.0 0.0 copy-start.1
  0.0 0.0 copy-start.2
  0.0 0.0 copy-start.3
  0.0 14.3 %attend.1.own_hbm = bf16[7,2304]{1,0:T(8,128)(2,1)} custom-call(s32[7]{0:T(128)} %lengths_hbm.1, f32[8]{0:T(128)} %lambdas_hbm.1, bf16[7,2304]{1,0:T(8,128)(2,1)} %tokens.1, bf16[2304]{0:T(1024)(128)(2,1)} %attn_gain_hbm.1, bf16[1,128]{1,0:T(2,128)(2,1)} %bitcast.17, bf16[2304,1024]{1,0:T(8,128)(2,1)} %query_hbm.1, bf16[2304,1024]{1,0:T(8,128)(2,1)} %key_hbm.1, ...), custom_call_target="tpu_custom_call" | custom-call | tf_op jit(solution)/shard_map/attend/pallas_call | solution.py:299
  14.3 0.6 collective-permute-start
  14.9 0.0 copy-done.5
  14.9 1.1 %collective-permute-done.other_part = bf16[7,2304]{1,0:T(8,128)(2,1)S(1)} collective-permute-done((bf16[7,2304]{1,0:T(8,128)(2,1)}, bf16[7,2304]{1,0:T(8,128)(2,1)S(1)}, u32[]{:S(2)}, u32[]{:S(2)}) %collective-permute-start) | collective-permute-done | bytes 32288 | tf_op jit(solution)/shard_map/ppermute | solution.py:543
  16.0 0.0 copy-done.1
  16.0 0.0 copy-done.2
  16.0 1.8 %prepare.1 = (bf16[7,2304]{1,0:T(8,128)(2,1)S(1)}, bf16[7,2304]{1,0:T(8,128)(2,1)S(1)}, bf16[16,48,128]{2,1,0:T(8,128)(2,1)}) custom-call(s32[1]{0:T(128)} %bitcast.index, bf16[7,2304]{1,0:T(8,128)(2,1)S(1)} %copy-done.1, bf16[7,2304]{1,0:T(8,128)(2,1)} %attend.1.own_hbm, bf16[7,2304]{1,0:T(8,128)(2,1)S(1)} %collective-permute-done.other_part, ...), custom_call_target="tpu_custom_call" | custom-call | tf_op jit(solution)/shard_map/prepare/pallas_call | solution.py:547
  17.8 8.3 %all-to-all-start = ((bf16[16,48,128]{2,1,0:T(8,128)(2,1)}), bf16[16,48,128]{2,1,0:T(8,128)(2,1)S(1)}, u32[]{:S(2)}, u32[]{:S(2)}) async-start(bf16[16,48,128]{2,1,0:T(8,128)(2,1)} %get-tuple-element.14), calls=%async_computation | async-start | bytes 393216 | tf_op jit(solution)/shard_map/all_to_all | solution.py:563
  26.1 0.0 copy-done.3
  26.1 0.4 shares.1
  26.5 8.6 %all-to-all-done.own = bf16[16,48,128]{2,1,0:T(8,128)(2,1)S(1)} async-done(((bf16[16,48,128]{2,1,0:T(8,128)(2,1)}), bf16[16,48,128]{2,1,0:T(8,128)(2,1)S(1)}, u32[]{:S(2)}, u32[]{:S(2)}) %all-to-all-start) | async-done | bytes 196640 | tf_op jit(solution)/shard_map/all_to_all | solution.py:563
  35.1 0.0 collective-permute-start.1
  35.1 1.4 %collective-permute-done.1.other = bf16[16,48,128]{2,1,0:T(8,128)(2,1)S(1)} collective-permute-done((bf16[16,48,128]{2,1,0:T(8,128)(2,1)S(1)}, bf16[16,48,128]{2,1,0:T(8,128)(2,1)S(1)}, u32[]{:S(2)}, u32[]{:S(2)}) %collective-permute-start.1) | collective-permute-done | bytes 196640 | tf_op jit(solution)/shard_map/ppermute | solution.py:578
  36.5 0.0 copy-start.4
  36.5 4.5 %expert.1 = (bf16[16,48,128]{2,1,0:T(8,128)(2,1)S(1)}, bf16[16,48,128]{2,1,0:T(8,128)(2,1)S(1)}) custom-call(s32[1]{0:T(128)} %bitcast.index, bf16[16,48,128]{2,1,0:T(8,128)(2,1)S(1)} %all-to-all-done.own, bf16[16,48,128]{2,1,0:T(8,128)(2,1)S(1)} %collective-permute-done.1.other, bf16[2304,512]{1,0:T(8,128)(2,1)} %bitcast.14, bf16[2304,512]{1,0:T(8,128)(2,1)} %bitcast.15, ...), custom_call_target="tpu_custom_call" | custom-call | tf_op jit(solution)/shard_map/expert/pallas_call | solution.py:579
  41.0 0.2 collective-permute-start.2
  41.2 0.0 copy-done.4
  41.2 0.4 fusion.4
  41.6 0.9 %collective-permute-done.2 = bf16[16,48,128]{2,1,0:T(8,128)(2,1)S(1)} collective-permute-done((bf16[16,48,128]{2,1,0:T(8,128)(2,1)S(1)}, bf16[16,48,128]{2,1,0:T(8,128)(2,1)S(1)}, u32[]{:S(2)}, u32[]{:S(2)}) %collective-permute-start.2) | collective-permute-done | bytes 196640 | tf_op jit(solution)/shard_map/ppermute | solution.py:602
  42.5 0.7 %add_convert_fusion = bf16[16,48,128]{2,1,0:T(8,128)(2,1)} fusion(bf16[16,48,128]{2,1,0:T(8,128)(2,1)S(1)} %collective-permute-done.2, bf16[16,48,128]{2,1,0:T(8,128)(2,1)S(1)} %get-tuple-element.18), kind=kLoop, calls=%fused_computation.1 | loop fusion | flops 393216 | bytes 589824 | tf_op jit(solution)/shard_map/convert_element_type | solution.py:604
  43.2 3.5 %all-to-all-start.1 = ((bf16[16,48,128]{2,1,0:T(8,128)(2,1)}), bf16[16,48,128]{2,1,0:T(8,128)(2,1)S(1)}, u32[]{:S(2)}, u32[]{:S(2)}) async-start(bf16[16,48,128]{2,1,0:T(8,128)(2,1)} %add_convert_fusion), calls=%async_computation.1 | async-start | bytes 393216 | tf_op jit(solution)/shard_map/all_to_all | solution.py:603
  46.8 0.0 copy-done
  46.8 2.5 %convolution_convert_fusion.own_shared = bf16[7,2304]{1,0:T(8,128)(2,1)S(1)} fusion(bf16[512,2304]{1,0:T(8,128)(2,1)S(1)} %copy-done, f32[7,512]{1,0:T(8,128)S(1)} %fusion.4, bf16[7,2304]{1,0:T(8,128)(2,1)S(1)} %get-tuple-element.15.after, bf16[2304,512]{1,0:T(8,128)(2,1)} %param.36), kind=kOutput, calls=%fused_computation | convolution fusion | flops 33067776 | bytes 4797440 | tf_op jit(solution)/shard_map/dot_general | solution.py:609
  49.3 0.2 collective-permute-start.3
  49.4 1.1 %collective-permute-done.3.other_shared = bf16[7,1152]{1,0:T(8,128)(2,1)S(1)} collective-permute-done((bf16[7,1152]{1,0:T(8,128)(2,1)S(1)}, bf16[7,1152]{1,0:T(8,128)(2,1)S(1)}, u32[]{:S(2)}, u32[]{:S(2)}) %collective-permute-start.3) | collective-permute-done | bytes 16160 | tf_op jit(solution)/shard_map/ppermute | solution.py:612
  50.5 5.2 %all-to-all-done.1.returned = bf16[16,48,128]{2,1,0:T(8,128)(2,1)S(1)} async-done(((bf16[16,48,128]{2,1,0:T(8,128)(2,1)}), bf16[16,48,128]{2,1,0:T(8,128)(2,1)S(1)}, u32[]{:S(2)}, u32[]{:S(2)}) %all-to-all-start.1) | async-done | bytes 196640 | tf_op jit(solution)/shard_map/all_to_all | solution.py:603
  55.7 1.1 %combine.1 = bf16[7,1152]{1,0:T(8,128)(2,1)} custom-call(s32[1]{0:T(128)} %bitcast.index, bf16[16,48,128]{2,1,0:T(8,128)(2,1)S(1)} %all-to-all-done.1.returned, bf16[16,72,48]{2,1,0:T(8,128)(2,1)S(1)} %get-tuple-element.20.high, bf16[16,72,48]{2,1,0:T(8,128)(2,1)S(1)} %get-tuple-element.21.low, bf16[7,2304]{1,0:T(8,128)(2,1)S(1)} %get-tuple-element.22.mixed, ...), custom_call_target="tpu_custom_call" | custom-call | tf_op jit(solution)/shard_map/combine/pallas_call | solution.py:613
  (2 shorter events, 0.0 us)
Async XLA Ops:
  0.0 46.8 %copy-start = (bf16[512,2304]{1,0:T(8,128)(2,1)S(1)}, bf16[512,2304]{1,0:T(8,128)(2,1)}, u32[]{:S(2)}) copy-start(bf16[512,2304]{1,0:T(8,128)(2,1)} %param.37) | copy-start | bytes 7077892
  0.0 14.9 %copy-start.5 = (bf16[2304]{0:T(1024)(128)(2,1)S(1)}, bf16[2304]{0:T(1024)(128)(2,1)}, u32[]{:S(2)}) copy-start(bf16[2304]{0:T(1024)(128)(2,1)} %param.31) | copy-start | bytes 13828
  0.0 16.0 %copy-start.1 = (bf16[7,2304]{1,0:T(8,128)(2,1)S(1)}, bf16[7,2304]{1,0:T(8,128)(2,1)}, u32[]{:S(2)}) copy-start(bf16[7,2304]{1,0:T(8,128)(2,1)} %tokens.1) | copy-start | bytes 96772
  0.0 16.0 %copy-start.2 = (s32[7,6]{1,0:T(8,128)S(1)}, s32[7,6]{1,0:T(8,128)}, u32[]{:S(2)}) copy-start(s32[7,6]{1,0:T(8,128)} %ids.3) | copy-start | bytes 508
  0.0 26.1 %copy-start.3 = (f32[7,6]{1,0:T(8,128)S(1)}, f32[7,6]{1,0:T(8,128)}, u32[]{:S(2)}) copy-start(f32[7,6]{1,0:T(8,128)} %weights.1) | copy-start | bytes 508
  14.3 1.6 %collective-permute-start = (bf16[7,2304]{1,0:T(8,128)(2,1)}, bf16[7,2304]{1,0:T(8,128)(2,1)S(1)}, u32[]{:S(2)}, u32[]{:S(2)}) collective-permute-start(bf16[7,2304]{1,0:T(8,128)(2,1)} %attend.1.own_hbm), channel_id=1, source_target_pairs={{0,1},{1,0},{2,3},{3,2},{4,5},{5,4},{6,7},{7,6},{8,9},{9,8},{10,11... | collective-permute-start | bytes 96776 | tf_op jit(solution)/shard_map/ppermute | solution.py:543
  17.8 17.3 %all-to-all-start = ((bf16[16,48,128]{2,1,0:T(8,128)(2,1)}), bf16[16,48,128]{2,1,0:T(8,128)(2,1)S(1)}, u32[]{:S(2)}, u32[]{:S(2)}) async-start(bf16[16,48,128]{2,1,0:T(8,128)(2,1)} %get-tuple-element.14), calls=%async_computation | async-start | bytes 393216 | tf_op jit(solution)/shard_map/all_to_all | solution.py:563
  35.1 1.4 %collective-permute-start.1 = (bf16[16,48,128]{2,1,0:T(8,128)(2,1)S(1)}, bf16[16,48,128]{2,1,0:T(8,128)(2,1)S(1)}, u32[]{:S(2)}, u32[]{:S(2)}) collective-permute-start(bf16[16,48,128]{2,1,0:T(8,128)(2,1)S(1)} %all-to-all-done.own), channel_id=1, source_target_pairs={{0,1},{1,0},{2,3},{3,2},{4,5},{5,4},{6,7},{7,6},{8,9},{9,8},{10,11... | collective-permute-start | bytes 589832 | tf_op jit(solution)/shard_map/ppermute | solution.py:578
  36.5 4.7 %copy-start.4 = (bf16[2304,512]{1,0:T(8,128)(2,1)S(1)}, bf16[2304,512]{1,0:T(8,128)(2,1)}, u32[]{:S(2)}) copy-start(bf16[2304,512]{1,0:T(8,128)(2,1)} %param.35) | copy-start | bytes 7077892
  41.0 1.5 %collective-permute-start.2 = (bf16[16,48,128]{2,1,0:T(8,128)(2,1)S(1)}, bf16[16,48,128]{2,1,0:T(8,128)(2,1)S(1)}, u32[]{:S(2)}, u32[]{:S(2)}) collective-permute-start(bf16[16,48,128]{2,1,0:T(8,128)(2,1)S(1)} %get-tuple-element.19), channel_id=1, source_target_pairs={{0,1},{1,0},{2,3},{3,2},{4,5},{5,4},{6,7},{7,6},{8,9},{9,8},{10,11... | collective-permute-start | bytes 589832 | tf_op jit(solution)/shard_map/ppermute | solution.py:602
  43.2 12.4 %all-to-all-start.1 = ((bf16[16,48,128]{2,1,0:T(8,128)(2,1)}), bf16[16,48,128]{2,1,0:T(8,128)(2,1)S(1)}, u32[]{:S(2)}, u32[]{:S(2)}) async-start(bf16[16,48,128]{2,1,0:T(8,128)(2,1)} %add_convert_fusion), calls=%async_computation.1 | async-start | bytes 393216 | tf_op jit(solution)/shard_map/all_to_all | solution.py:603
  49.3 1.2 %collective-permute-start.3 = (bf16[7,1152]{1,0:T(8,128)(2,1)S(1)}, bf16[7,1152]{1,0:T(8,128)(2,1)S(1)}, u32[]{:S(2)}, u32[]{:S(2)}) collective-permute-start(bf16[7,1152]{1,0:T(8,128)(2,1)S(1)} %constant_dynamic-slice_fusion), channel_id=1, source_target_pairs={{0,1},{1,0},{2,3},{3,2},{4,5},{5,4},{6,7},{7,6},{8,9},{9,8},{10,11... | collective-permute-start | bytes 48392 | tf_op jit(solution)/shard_map/ppermute | solution.py:612
